TPU v7x, 768 devices: a whole 4x8x12 slice. The times are simulated.
768 devices in a mesh: fs: 96 (over z, y), tp: 8 (over x, core).
Axes of the slice: x: 4, y: 8, z: 12, core: 2. Of those that a mesh axis runs over, the one named last changes fastest.
Arguments:
- inputs: bfloat16 [49152, 2112], P('fs', 'tp'), may hold values from -20 to 20
- w_conv_up: bfloat16 [2112, 2816], P('fs', 'tp'), may hold values from -0.125 to 0.125
- w_gate_up: bfloat16 [2112, 2816], P('fs', 'tp'), may hold values from -0.125 to 0.125
- w_down: bfloat16 [2816, 2112], P('tp', 'fs'), may hold values from -0.109375 to 0.109375
- taps: float32 [3, 2816], replicated, may hold values from -3 to 3
- conv_bias: float32 [2816], replicated, may hold values from -3 to 3
- cotangent: bfloat16 [49152, 2112], P('fs', 'tp'), may hold values from -6 to 6
Outputs:
- grad_inputs: bfloat16 [49152, 2112], P('fs', 'tp')
- grad_conv_up: float32 [2112, 2816], P('fs', 'tp')
- unit_norms: float32 [2816], P('tp')
- grad_taps: float32 [3, 2816], replicated
- grad_bias: float32 [2816], replicated
All inputs are finite; a program needn't handle non-finite values.
Results may differ from a plain program's by a relative error of at most 0.018.
Values may be sent and summed in bfloat16 or wider, within the bound.
No kernel may reach another device: no remote copies, remote signals or barrier semaphores. Data moves between devices by JAX's collectives and lax.ppermute only.
A program may use at most 64 MiB of HBM per device.

v0:
```python
import math

import jax
import jax.numpy as jnp
from jax import lax
from jax.sharding import Mesh
from jax.sharding import PartitionSpec as P

TAPS = 3
FS = ("fs_0", "fs_1")


def rows_first(arrays, axis, dims):
    turned = [jnp.moveaxis(a, dim, 0) for a, dim in zip(arrays, dims)]
    both = jnp.concatenate([t.reshape(len(t), -1) for t in turned], axis=1)
    result, at, outs = (lax.all_gather(both, axis, axis=0, tiled=True), 0, [])
    for t, dim in zip(turned, dims):
        section = result[:, at : at + t[0].size].reshape(-1, *t.shape[1:])
        outs.append(jnp.moveaxis(section, 0, dim))
        at += t[0].size
    return tuple(outs)


def sent_together(arrays, axis, dim, along):
    ends, at = ([], 0)
    for a in arrays[:-1]:
        at += a.shape[along]
        ends.append(at)
    both = jnp.concatenate(arrays, axis=along)
    return tuple(jnp.split(lax.all_gather(both, axis, axis=dim, tiled=True), ends, axis=along))


def in_order(parts, dim):
    lengths = list(parts.shape[1:])
    lengths[dim] *= parts.shape[0]
    return jnp.moveaxis(parts, 0, dim).reshape(lengths)


def stacked_from(value, axes, turns):
    parts = value[None]
    for k in turns:
        parts = lax.all_gather(parts, axes[k], axis=0, tiled=True)
    block = [lax.axis_size(axes[k]) for k in reversed(turns)]
    parts = parts.reshape(*block, *value.shape)
    turned = sorted(range(len(turns)), key=lambda place: turns[len(turns) - 1 - place])
    return parts.transpose(*turned, *range(len(turns), parts.ndim)).reshape(-1, *value.shape)


def gather_axes(value, axes, turns, dim):
    return in_order(stacked_from(value, axes, turns), dim)


def shifted(block, axis, distance):
    devices = range(lax.axis_size(axis))
    route = [(i - distance, i) for i in devices if i - distance in devices]
    return lax.ppermute(block, axis, route)


def reduced_to_own(parts, axes, turns):
    inside = parts.shape[1:]
    parts = parts.reshape(*(lax.axis_size(a) for a in axes), *inside)
    parts = jnp.moveaxis(parts, turns, range(len(axes))).reshape(-1, *inside)
    for k in turns:
        parts = lax.psum_scatter(parts, axes[k], scatter_dimension=0, tiled=True)
    return parts[0]


def split_up(value, dim, count):
    lengths = value.shape
    parts = value.reshape(*lengths[:dim], count, lengths[dim] // count, *lengths[dim + 1 :])
    return jnp.moveaxis(parts, dim, 0)


def scatter_axes(value, axes, turns, dim):
    count = lax.axis_size(axes)
    return reduced_to_own(split_up(value, dim, count), axes, turns)


def by_axis(value, axes):
    for axis in axes:
        value = lax.psum(value, axis)
    return value


def from_everyone(value, axis):
    copies = jnp.broadcast_to(value, (lax.axis_size(axis), *value.shape))
    return lax.all_to_all(copies, axis, split_axis=0, concat_axis=0, tiled=True)


def gathered_copies(value, axis, dim):
    return in_order(from_everyone(value, axis), dim)


def gelu_parts(value):
    normal_cdf = 0.5 * (1.0 + jax.scipy.special.erf(value / math.sqrt(2.0)))
    density = jnp.exp(-0.5 * value * value) / math.sqrt(2.0 * math.pi)
    return (value * normal_cdf, normal_cdf + value * density)


def per_device(inputs, w_conv_up, w_gate_up, w_down, taps, conv_bias, cotangent):
    span = TAPS - 1
    rows = inputs.shape[0]
    width = w_conv_up.shape[1]
    col_start = lax.axis_index("tp") * width
    taps_own = lax.dynamic_slice_in_dim(taps, col_start, width, 1)
    bias_own = lax.dynamic_slice_in_dim(conv_bias, col_start, width, 0)
    features, cot_full = rows_first((inputs, cotangent), "tp", (1, 1))
    conv_weight, gate_weight = sent_together((w_conv_up, w_gate_up), FS, 0, 1)
    columns = cot_full
    d_hidden = lax.dot_general(
        columns,
        gather_axes(w_down, FS, (0, 1), 1),
        (((1,), (1,)), ((), ())),
        preferred_element_type=jnp.float32,
    ).astype(jnp.bfloat16)
    up_a = jnp.dot(features, conv_weight, preferred_element_type=jnp.float32).astype(jnp.bfloat16)
    up_b = jnp.dot(features, gate_weight, preferred_element_type=jnp.float32).astype(jnp.bfloat16)
    earlier = shifted(up_a[rows - span :], FS, 1)
    extended = jnp.concatenate([earlier, up_a], 0).astype(jnp.float32)
    conv_out = bias_own[None, :] + sum(
        (taps_own[i][None, :] * extended[i : i + rows] for i in range(TAPS))
    )
    gelu_value, gelu_slope = gelu_parts(conv_out)
    hidden_grad = d_hidden.astype(jnp.float32)
    d_conv = hidden_grad * up_b.astype(jnp.float32) * gelu_slope
    d_up_b = (hidden_grad * gelu_value).astype(jnp.bfloat16)
    later = shifted(d_conv[:span], FS, -1)
    d_extended = jnp.concatenate([d_conv, later], 0)
    d_up_a = sum(
        (taps_own[i][None, :] * d_extended[span - i : span - i + rows] for i in range(TAPS))
    ).astype(jnp.bfloat16)
    tap_terms = [jnp.sum(d_conv * extended[i : i + rows], axis=0) for i in range(TAPS)]
    column_part = jnp.stack(tap_terms + [jnp.sum(d_conv, axis=0)], 0)
    contract = (((1,), (1,)), ((), ()))
    partial_sum = lax.dot_general(d_up_a, conv_weight, contract, preferred_element_type=jnp.float32)
    partial_sum = partial_sum + lax.dot_general(
        d_up_b, gate_weight, contract, preferred_element_type=jnp.float32
    )
    grad_inputs = lax.psum_scatter(
        partial_sum.astype(jnp.bfloat16), "tp", scatter_dimension=1, tiled=True
    )
    columns = features
    grad_conv_up = scatter_axes(
        lax.dot_general(
            columns, d_up_a, (((0,), (0,)), ((), ())), preferred_element_type=jnp.float32
        ),
        FS,
        (1, 0),
        0,
    )
    squares = jnp.sum(grad_conv_up * grad_conv_up, axis=0)
    column_totals, unit_norms = (by_axis(column_part, FS), by_axis(squares, FS))
    full_columns = gathered_copies(column_totals, "tp", 1)
    return (grad_inputs, grad_conv_up, unit_norms, full_columns[:TAPS], full_columns[TAPS])


def solution(mesh):
    finer = Mesh(mesh.devices.reshape(12, 8, mesh.shape["tp"]), ("fs_0", "fs_1", "tp"))
    placed = (P(FS, "tp"), P(FS, "tp"), P(FS, "tp"), P("tp", FS), P(), P(), P(FS, "tp"))
    return jax.shard_map(
        per_device,
        mesh=finer,
        in_specs=placed,
        out_specs=(P(FS, "tp"), P(FS, "tp"), P("tp"), P(), P()),
        check_vma=False,
    )
```

profile of v0, /device:TPU:6, one launch (start us, length us, event | category | flops | bytes accessed | tf_op | source)
XLA Modules:
  0.0 454.4 jit_solution(14301582016648878418)
XLA Ops:
  7.2 35.4 %all-gather.1 = bf16[12,352,22]{1,2,0:T(8,128)(2,1)} all-gather(bf16[1,352,22]{1,2,0:T(8,128)(2,1)} %bitcast.34), channel_id=2, replica_groups=mesh['fs_0'=12,'fs_1'=8,'tp'=8] {'fs_0'}, dimensions={0}, use_global_device_ids=true | all-gather | bytes 201344 | tf_op jit(solution)/shard_map/all_gather | solution.py:42
  42.7 1.4 maximum_bitcast_fusion
  44.2 1.9 pad_maximum_fusion.1
  47.8 34.9 %all-gather.9.cloned.1.call-done = bf16[96,352,22]{1,2,0:T(8,128)(2,1)} async-done(((bf16[12,352,22]{1,2,0:T(8,128)(2,1)}), bf16[96,352,22]{1,2,0:T(8,128)(2,1)}) %all-gather.9.cloned.1.call-update) | async-done | bytes 1486864 | tf_op jit(solution)/shard_map/all_gather | solution.py:42
  82.7 2.0 copy.30
  85.4 2.2 reshape.29
  87.5 123.8 %all-gather.11.cloned.1.call-done = bf16[96,22,704]{2,1,0:T(8,128)(2,1)} async-done(((bf16[1,22,704]{2,1,0:T(8,128)(2,1)}), bf16[96,22,704]{2,1,0:T(8,128)(2,1)}) %all-gather.11.cloned.1.call-update) | async-done | bytes 2973712 | tf_op jit(solution)/shard_map/all_gather | solution.py:30
  211.3 4.3 reshape.35
  215.6 33.1 %all-gather.7.cloned.1.call-done = bf16[2112,1024]{1,0:T(8,128)(2,1)} async-done(((bf16[264,1024]{1,0:T(8,128)(2,1)}), bf16[2112,1024]{1,0:T(8,128)(2,1)}) %all-gather.7.cloned.1.call-update) | async-done | bytes 4325392 | tf_op jit(solution)/shard_map/all_gather | solution.py:16
  248.7 2.8 fusion.34
  251.7 3.4 collective-permute-start
  258.2 1.9 fusion.29
  261.4 7.2 %collective-permute-done.1 = f32[2,352]{0,1:T(8,128)S(1)} collective-permute-done((f32[2,352]{0,1:T(8,128)S(1)}, f32[2,352]{0,1:T(8,128)S(1)}, u32[]{:S(2)}, u32[]{:S(2)}) %collective-permute-start.1) | collective-permute-done | bytes 2848 | tf_op jit(solution)/shard_map/ppermute | solution.py:56
  268.6 1.4 multiply_reduce_fusion.2
  270.7 1.3 fusion.3
  272.1 2.3 reshape_reshape.3
  274.4 4.0 copy.26
  278.5 57.6 %reduce-scatter.8.cloned.1.call-done = f32[12,22,352]{2,1,0:T(8,128)} async-done(((f32[96,22,352]{2,1,0:T(8,128)}), f32[12,22,352]{2,1,0:T(8,128)}) %reduce-scatter.8.cloned.1.call-update) | async-done | bytes 371728 | tf_op jit(solution)/shard_map/reduce_scatter | solution.py:64
  336.4 2.4 fusion.11
  338.8 2.8 fusion
  341.6 55.4 %reduce-scatter.10.cloned.1.call-done = f32[1,22,352]{2,1,0:T(8,128)} async-done(((f32[12,22,352]{2,1,0:T(8,128)}), f32[1,22,352]{2,1,0:T(8,128)}) %reduce-scatter.10.cloned.1.call-update) | async-done | bytes 30992
  397.8 22.3 %all-reduce.1 = (f32[352]{0:T(512)S(1)}, f32[4,352]{1,0:T(4,128)S(1)}) all-reduce(f32[352]{0:T(512)S(1)} %multiply_reduce_fusion.3, f32[4,352]{1,0:T(4,128)S(1)} %pad_maximum_fusion.2), channel_id=1, replica_groups=mesh['fs_0'=12,'fs_1'=8,'tp'=8] {'fs_0'}, use_global_device_ids=true, to_apply=%region_4.0 | all-reduce | flops 1760 | bytes 14080 | tf_op jit(solution)/shard_map/psum | solution.py:81
  420.2 17.9 %all-reduce.2 = (f32[352]{0:T(512)}, f32[4,352]{1,0:T(4,128)S(1)}) all-reduce(f32[352]{0:T(512)S(1)} %get-tuple-element.12, f32[4,352]{1,0:T(4,128)S(1)} %get-tuple-element.13), channel_id=1, replica_groups=mesh['fs_0'=12,'fs_1'=8,'tp'=8] {'fs_1'}, use_global_device_ids=true, to_apply=%region_5.0 | all-reduce | flops 1760 | bytes 14080 | tf_op jit(solution)/shard_map/psum | solution.py:81
  438.1 8.1 %all_to_all.5 = f32[8,4,352]{2,1,0:T(4,128)S(1)} all-to-all(f32[8,4,352]{2,1,0:T(4,128)S(1)} %broadcast_in_dim.8), channel_id=1, replica_groups=mesh['fs_0'=12,'fs_1'=8,'tp'=8] {'tp'}, dimensions={0} | all-to-all | bytes 90112 | tf_op jit(solution)/shard_map/all_to_all | solution.py:87
  (52 shorter events, 10.3 us)
Async XLA Ops:
  7.2 75.6 %all-gather.9.cloned.1.call-start = ((), (), s32[]{:S(2)}) async-start(), calls=%async_computation.5 | async-start | bytes 1990656 | tf_op jit(solution)/shard_map/all_gather | solution.py:42
  42.6 168.7 %all-gather.11.cloned.1.call-start = ((), (), s32[]{:S(2)}) async-start(), calls=%async_computation.8 | async-start | bytes 3575808 | tf_op jit(solution)/shard_map/all_gather | solution.py:30
  44.1 204.6 %all-gather.7.cloned.1.call-start = ((), (), s32[]{:S(2)}) async-start(), calls=%async_computation.4 | async-start | bytes 4866048 | tf_op jit(solution)/shard_map/all_gather | solution.py:16
  46.1 290.0 %reduce-scatter.8.cloned.1.call-start = ((), (), s32[]{:S(2)}) async-start(), calls=%async_computation.7 | async-start | bytes 3981312 | tf_op jit(solution)/shard_map/reduce_scatter | solution.py:64
  215.6 42.6 %copy-start = (bf16[2112,704]{1,0:T(8,128)(2,1)}, bf16[2112,704]{1,0:T(8,128)(2,1)S(1)}, u32[]{:S(2)}) copy-start(bf16[2112,704]{1,0:T(8,128)(2,1)S(1)} %reshape.35) | copy-start | bytes 8921092
  248.7 6.3 %copy-start.3 = (bf16[2112,1024]{1,0:T(8,128)(2,1)S(1)}, bf16[2112,1024]{1,0:T(8,128)(2,1)}, u32[]{:S(2)}) copy-start(bf16[2112,1024]{1,0:T(8,128)(2,1)} %all-gather.7.cloned.1.call-done) | copy-start | bytes 12976132
  248.7 6.3 %copy-start.6 = (bf16[352,2112]{0,1:T(8,128)(2,1)S(1)}, bf16[352,2112]{0,1:T(8,128)(2,1)}, u32[]{:S(2)}) copy-start(bf16[352,2112]{0,1:T(8,128)(2,1)} %reshape.29) | copy-start | bytes 4460548
  251.7 5.7 %collective-permute-start = (bf16[2,352]{0,1:T(8,128)(2,1)S(1)}, bf16[2,352]{0,1:T(8,128)(2,1)S(1)}, u32[]{:S(2)}, u32[]{:S(2)}) collective-permute-start(bf16[2,352]{0,1:T(8,128)(2,1)S(1)} %slice.69), channel_id=1, source_target_pairs={{0,8},{8,16},{16,24},{24,32},{32,40},{40,48},{48,56},{56,64},{64,7... | collective-permute-start | bytes 4232 | tf_op jit(solution)/shard_map/ppermute | solution.py:56
  256.2 3.9 copy-start.7
  258.2 1.9 copy-start.4
  260.1 8.5 %collective-permute-start.1 = (f32[2,352]{0,1:T(8,128)S(1)}, f32[2,352]{0,1:T(8,128)S(1)}, u32[]{:S(2)}, u32[]{:S(2)}) collective-permute-start(f32[2,352]{0,1:T(8,128)S(1)} %slice.73), channel_id=1, source_target_pairs={{8,0},{16,8},{24,16},{32,24},{40,32},{48,40},{56,48},{64,56},{72,6... | collective-permute-start | bytes 8456 | tf_op jit(solution)/shard_map/ppermute | solution.py:56
  270.0 0.7 copy-start.2
  278.4 58.0 %copy-start.1 = (bf16[2112,704]{1,0:T(8,128)(2,1)S(1)}, bf16[2112,704]{1,0:T(8,128)(2,1)}, u32[]{:S(2)}) copy-start(bf16[2112,704]{1,0:T(8,128)(2,1)} %copy-done) | copy-start | bytes 8921092
  278.4 118.6 %reduce-scatter.10.cloned.1.call-start = ((), (), s32[]{:S(2)}) async-start(), calls=%async_computation.9 | async-start | bytes 479232
  336.1 111.4 %reduce-scatter.6.cloned.1.call-start = ((), (), s32[]{:S(2)}) async-start(), calls=%async_computation.6 | async-start | bytes 2433024 | tf_op jit(solution)/shard_map/reduce_scatter | solution.py:139
  336.4 2.4 copy-start.5
  336.4 2.4 copy-start.8
Sparse Core Ops, SparseCore 0:
  42.7 39.9 all-gather.8
  87.0 124.2 all-gather.10
  213.7 34.9 all-gather.6
  278.5 57.5 reduce-scatter.7
  339.6 57.3 reduce-scatter.9
  400.6 36.9 reduce-scatter.5
where the time goes:
time: 457 us; the launch traced here: 454 us
  waiting for transfers between devices  313 us (68%)
  blocking collectives  83.6 us (18%)
  local copies, waits for them, and re-layouts  19.4 us (4%)
  between operations  14.4 us (3%)
  matrix products  12.2 us (3%)
  other arithmetic  6.38 us (1%)
  starting transfers between devices  5.11 us (1%)
    all_gather x1, waiting for transfers between devices, sent_together(): lax.all_gather(both, axis, axis=dim, tiled=True)  124 us
    reduce_scatter x1, waiting for transfers between devices, reduced_to_own(): parts = lax.psum_scatter(parts, axes[k], scatter_dimension=0, tiled=True)  57.6 us
    unnamed x7, waiting for transfers between devices  55.5 us
    psum x2, blocking collectives, by_axis(): value = lax.psum(value, axis)  40.2 us
    all_gather x1, blocking collectives, stacked_from(): parts = lax.all_gather(parts, axes[k], axis=0, tiled=True)  35.4 us
    all_gather x1, waiting for transfers between devices, stacked_from(): parts = lax.all_gather(parts, axes[k], axis=0, tiled=True)  34.9 us
    all_gather x1, waiting for transfers between devices, rows_first(): result, at, outs = (lax.all_gather(both, axis, axis=0, tiled=True), 0, [])  33.1 us
  transfers between devices with their start and end apart: 8, of which 7 were waited for; matrix products, arithmetic and copies ran while one was open for 5% of the time, Pallas kernels for 0%

commit v1 on v0

v1 whole, which is shorter than its diff:
```python
import math

import jax
import jax.numpy as jnp
from jax import lax
from jax.sharding import Mesh
from jax.sharding import PartitionSpec as P

TAPS = 3
FS = ("z", "y")
TP = ("x", "c")
LANES = 128


def up_to(n, m):
    return -(-n // m) * m


def pad_to(value, dim, length):
    widths = [(0, 0)] * value.ndim
    widths[dim] = (0, length - value.shape[dim])
    return jnp.pad(value, widths)


def broadcast(value, axes):
    copies = jnp.broadcast_to(value, (lax.axis_size(axes), *value.shape))
    return lax.all_to_all(copies, axes, split_axis=0, concat_axis=0, tiled=True)


def neighbour(block, distance):
    devices = range(lax.axis_size(FS))
    route = [(i - distance, i) for i in devices if i - distance in devices]
    return lax.ppermute(block, FS, route)


def gelu_parts(value):
    normal_cdf = 0.5 * (1.0 + jax.scipy.special.erf(value / math.sqrt(2.0)))
    density = jnp.exp(-0.5 * value * value) / math.sqrt(2.0 * math.pi)
    return (value * normal_cdf, normal_cdf + value * density)


def per_device(inputs, w_conv_up, w_gate_up, w_down, taps, conv_bias, cotangent):
    span = TAPS - 1
    nz, ny = lax.axis_size("z"), lax.axis_size("y")
    ntp = lax.axis_size(TP)
    rows, feats = inputs.shape
    wrows, width = w_conv_up.shape
    wpad, fpad = up_to(wrows, 8), up_to(width, LANES)
    groups = feats // wrows
    f32 = jnp.float32

    before = neighbour(inputs[rows - span :], 1)
    after = neighbour(jnp.concatenate([inputs[:span], cotangent[:span]], 0), -1)

    packed = jnp.concatenate(
        [pad_to(w, 1, fpad) for w in (w_conv_up, w_gate_up, w_down.T)], axis=1
    )
    packed = pad_to(packed, 0, wpad)
    over_y = broadcast(packed, "y").reshape(ny * wpad, 3 * fpad)
    weights = lax.all_gather(over_y, "z", axis=0, tiled=True)

    halo = pad_to(jnp.concatenate([before, after], 0), 0, LANES)
    acts = jnp.concatenate([inputs, halo, cotangent], 0).T
    acts = pad_to(acts.reshape(groups, wrows, -1), 1, wpad)
    acts, over_y = lax.optimization_barrier((acts, over_y))
    tokens = acts.shape[-1]
    over_x = broadcast(acts, "x")
    over_tp = broadcast(over_x, "c")
    whole = jnp.moveaxis(over_tp, 0, 1).reshape(nz * ny, wpad, tokens)
    by_y = whole[:, :, :rows].reshape(nz, ny, wpad, rows)
    by_y = jnp.moveaxis(by_y, 0, 1).reshape(ny * nz * wpad, rows)
    whole = whole.reshape(nz * ny * wpad, tokens)

    start = lax.axis_index(TP) * width
    taps_own = pad_to(lax.dynamic_slice_in_dim(taps, start, width, 1), 1, fpad)
    bias_own = pad_to(lax.dynamic_slice_in_dim(conv_bias, start, width, 0), 0, fpad)

    def over_rows(a, b):
        return lax.dot_general(a, b, (((0,), (0,)), ((), ())), preferred_element_type=f32)

    ups = over_rows(whole[:, : rows + LANES], weights[:, : 2 * fpad]).astype(jnp.bfloat16)
    d_hid = over_rows(whole[:, rows:], weights[:, 2 * fpad :]).astype(jnp.bfloat16)
    up_a, up_b = ups[:, :fpad].astype(f32), ups[:, fpad:].astype(f32)
    first = rows + span
    extended = jnp.concatenate([up_a[rows:first], up_a[:rows], up_a[first : first + span]], 0)
    gate = jnp.concatenate([up_b[:rows], up_b[first : first + span]], 0)
    hidden_grad = jnp.concatenate(
        [d_hid[LANES:], d_hid[2 * span : 3 * span]], 0
    ).astype(f32)
    reach = rows + span
    conv_out = bias_own[None, :] + sum(
        (taps_own[i][None, :] * extended[i : i + reach] for i in range(TAPS))
    )
    gelu_value, gelu_slope = gelu_parts(conv_out)
    d_conv = hidden_grad * gate * gelu_slope
    d_up_b = (hidden_grad[:rows] * gelu_value[:rows]).astype(jnp.bfloat16)
    d_up_a = sum(
        (taps_own[i][None, :] * d_conv[span - i : span - i + rows] for i in range(TAPS))
    ).astype(jnp.bfloat16)
    own = d_conv[:rows]
    sums = [jnp.sum(own * extended[i : i + rows], axis=0) for i in range(TAPS)]
    sums.append(jnp.sum(own, axis=0))

    both = jnp.concatenate([d_up_a, d_up_b], 1)
    partial = lax.dot_general(
        weights[:, : 2 * fpad], both, (((1,), (1,)), ((), ())), preferred_element_type=f32
    ).astype(jnp.bfloat16)
    grad_in = lax.psum_scatter(partial, TP, scatter_dimension=0, tiled=True)
    grad_in = grad_in.reshape(groups, wpad, rows)[:, :wrows].reshape(feats, rows).T

    part = jnp.dot(by_y, d_up_a, preferred_element_type=f32).astype(jnp.bfloat16)
    part = part.reshape(ny, nz * wpad, fpad)
    part = lax.all_to_all(part, "y", split_axis=0, concat_axis=0, tiled=True)
    part = jnp.sum(part.astype(f32), axis=0).reshape(nz, wpad, fpad)
    part = lax.all_to_all(part, "z", split_axis=0, concat_axis=0, tiled=True)
    grad_up = jnp.sum(part, axis=0)

    small = jnp.stack([jnp.sum(grad_up * grad_up, axis=0)] + sums, 0)
    small = pad_to(small, 0, 8)
    small = jnp.sum(broadcast(small, "z"), axis=0)
    small = broadcast(small, ("y", *TP)).reshape(ny, ntp, 8, fpad)
    small = jnp.sum(small, axis=0)[:, :, :width]
    unit_norms = lax.dynamic_index_in_dim(small, lax.axis_index(TP), 0, keepdims=False)[0]
    columns = jnp.moveaxis(small[:, 1 : TAPS + 2], 0, 1).reshape(TAPS + 1, ntp * width)
    return (grad_in, grad_up[:wrows, :width], unit_norms, columns[:TAPS], columns[TAPS])


def solution(mesh):
    finer = Mesh(mesh.devices.reshape(12, 8, 4, 2), ("z", "y", "x", "c"))
    placed = (P(FS, TP), P(FS, TP), P(FS, TP), P(TP, FS), P(), P(), P(FS, TP))
    return jax.shard_map(
        per_device,
        mesh=finer,
        in_specs=placed,
        out_specs=(P(FS, TP), P(FS, TP), P(TP), P(), P()),
        check_vma=False,
    )
```

time: 457 us -> 257 us (0.56)
  waiting for transfers between devices: 313 us -> 129 us
  blocking collectives: 83.6 us -> 47 us
  starting transfers between devices: 5.11 us -> 30.8 us
  local copies, waits for them, and re-layouts: 19.4 us -> 14.5 us
    all_gather x3 -> x1, waiting for transfers between devices: 192 us -> 21 us  [per_device(): weights = lax.all_gather(over_y, 'z', axis=0, tiled=True)]
    all_to_all x0 -> x4, waiting for transfers between devices: none -> 107 us  [the longest x2 46.9 us: broadcast(): return lax.all_to_all(copies, axes, split_axis=0, concat_axis=0, tiled=True)]
    reduce_scatter x2 -> x1, waiting for transfers between devices: 57.6 us -> 0.02 us  [per_device(): grad_in = lax.psum_scatter(partial, TP, scatter_dimension=0, tiled=True)]
    unnamed x7 -> x2, waiting for transfers between devices: 55.5 us -> 0.03 us
    psum x2 -> x0, blocking collectives: 40.2 us -> none  [by_axis(): value = lax.psum(value, axis)]
    all_to_all x1 -> x3, blocking collectives: 8.05 us -> 47 us  [broadcast(): return lax.all_to_all(copies, axes, split_axis=0, concat_axis=0, tiled=True)]
    all_gather x1 -> x0, blocking collectives: 35.4 us -> none  [stacked_from(): parts = lax.all_gather(parts, axes[k], axis=0, tiled=True)]
    all_to_all x0 -> x4, starting transfers between devices: none -> 24.9 us  [the longest x2 11.2 us: broadcast(): return lax.all_to_all(copies, axes, split_axis=0, concat_axis=0, tiled=True)]
  transfers between devices with their start and end apart: 8 -> 8, of which waited for: 7 -> 6; matrix products, arithmetic and copies ran while one was open for 5% -> 6% of each run, Pallas kernels for 0% -> 0%
where the time goes in v1:
time: 257 us; the launch traced here: 255 us
  waiting for transfers between devices  129 us (50%)
  blocking collectives  47 us (18%)
  starting transfers between devices  30.8 us (12%)
  matrix products  15 us (6%)
  local copies, waits for them, and re-layouts  14.5 us (6%)
  between operations  14.5 us (6%)
  other arithmetic  4.37 us (2%)
    all_to_all x3, blocking collectives, broadcast(): return lax.all_to_all(copies, axes, split_axis=0, concat_axis=0, tiled=True)  47 us
    all_to_all x2, waiting for transfers between devices, broadcast(): return lax.all_to_all(copies, axes, split_axis=0, concat_axis=0, tiled=True)  46.9 us
    all_to_all x1, waiting for transfers between devices, per_device(): part = lax.all_to_all(part, 'y', split_axis=0, concat_axis=0, tiled=True)  38.4 us
    all_to_all x1, waiting for transfers between devices, per_device(): part = lax.all_to_all(part, 'z', split_axis=0, concat_axis=0, tiled=True)  21.2 us
    all_gather x1, waiting for transfers between devices, per_device(): weights = lax.all_gather(over_y, 'z', axis=0, tiled=True)  21 us
    all_to_all x2, starting transfers between devices, broadcast(): return lax.all_to_all(copies, axes, split_axis=0, concat_axis=0, tiled=True)  11.2 us
    all_to_all x1, starting transfers between devices, per_device(): part = lax.all_to_all(part, 'y', split_axis=0, concat_axis=0, tiled=True)  6.87 us
    all_to_all x1, starting transfers between devices, per_device(): part = lax.all_to_all(part, 'z', split_axis=0, concat_axis=0, tiled=True)  6.82 us
  transfers between devices with their start and end apart: 8, of which 6 were waited for; matrix products, arithmetic and copies ran while one was open for 6% of the time, Pallas kernels for 0%

profile of v1, /device:TPU:6, one launch (start us, length us, event | category | flops | bytes accessed | tf_op | source)
XLA Modules:
  0.0 255.1 jit_solution(11538698418737824227)
XLA Ops:
  8.1 22.7 %all_to_all.35 = bf16[8,24,1152]{2,1,0:T(8,128)(2,1)} all-to-all(bf16[8,24,1152]{2,1,0:T(8,128)(2,1)S(1)} %broadcast_in_dim.16), channel_id=1, replica_groups=mesh['z'=12,'y'=8,'x'=4,'c'=2] {'y'}, dimensions={0} | all-to-all | bytes 884736 | tf_op jit(solution)/shard_map/all_to_all | solution.py:27
  31.9 1.0 fusion.58
  33.0 1.3 collective-permute-start.1
  34.4 4.6 %collective-permute-start = (bf16[2,264]{1,0:T(2,128)(2,1)S(1)}, bf16[2,264]{1,0:T(2,128)(2,1)S(1)}, u32[]{:S(2)}, u32[]{:S(2)}) collective-permute-start(bf16[2,264]{1,0:T(2,128)(2,1)S(1)} %copy.32), channel_id=1, source_target_pairs={{0,8},{8,16},{16,24},{24,32},{32,40},{40,48},{48,56},{56,64},{64,7... | collective-permute-start | bytes 3176 | tf_op jit(solution)/shard_map/ppermute | solution.py:33
  39.0 1.3 collective-permute-done
  40.7 1.7 broadcast_in_dim.17
  42.4 5.8 %all-to-all-start.1 = ((bf16[4,12,24,1152]{3,2,1,0:T(8,128)(2,1)}), bf16[4,12,24,1152]{3,2,1,0:T(8,128)(2,1)S(1)}, u32[]{:S(2)}, u32[]{:S(2)}) async-start(bf16[4,12,24,1152]{3,2,1,0:T(8,128)(2,1)} %broadcast_in_dim.17), calls=%async_computation.1 | async-start | bytes 5308416 | tf_op jit(solution)/shard_map/all_to_all | solution.py:27
  49.1 25.5 %all-to-all-done.1 = bf16[4,12,24,1152]{3,2,1,0:T(8,128)(2,1)S(1)} async-done(((bf16[4,12,24,1152]{3,2,1,0:T(8,128)(2,1)}), bf16[4,12,24,1152]{3,2,1,0:T(8,128)(2,1)S(1)}, u32[]{:S(2)}, u32[]{:S(2)}) %all-to-all-start.1) | async-done | bytes 2654240 | tf_op jit(solution)/shard_map/all_to_all | solution.py:27
  75.0 8.0 %all_to_all.36 = bf16[2,4,12,24,1152]{4,3,2,1,0:T(8,128)(2,1)S(1)} all-to-all(bf16[2,4,12,24,1152]{4,3,2,1,0:T(8,128)(2,1)S(1)} %broadcast_in_dim.18), channel_id=1, replica_groups=mesh['z'=12,'y'=8,'x'=4,'c'=2] {'c'}, dimensions={0} | all-to-all | bytes 10616832 | tf_op jit(solution)/shard_map/all_to_all | solution.py:27
  83.5 2.3 copy-done.1
  86.2 21.0 %all-gather.2.cloned.1.call-done = bf16[2304,1152]{1,0:T(8,128)(2,1)} async-done(((bf16[192,1152]{1,0:T(8,128)(2,1)}), bf16[2304,1152]{1,0:T(8,128)(2,1)}) %all-gather.2.cloned.1.call-update) | async-done | bytes 5308432 | tf_op jit(solution)/shard_map/all_gather | solution.py:60
  107.2 4.2 %fusion.12 = bf16[640,384]{1,0:T(8,128)(2,1)S(1)} fusion(bf16[2304,1152]{1,0:T(8,128)(2,1)} %all-gather.2.cloned.1.call-done, bf16[2304,1152]{1,0:T(8,128)(2,1)} %bitcast.27), kind=kOutput, calls=%fused_computation.16 | convolution fusion | flops 1132707840 | bytes 5210112 | tf_op jit(solution)/shard_map/dot_general | solution.py:79
  112.4 2.6 %fusion.7 = bf16[640,768]{1,0:T(8,128)(2,1)S(1)} fusion(bf16[2304,1152]{1,0:T(8,128)(2,1)S(1)} %copy-done.8, bf16[2304,1152]{1,0:T(8,128)(2,1)S(1)} %bitcast.30), kind=kOutput, calls=%fused_computation.15 | convolution fusion | flops 2265415680 | bytes 7471104 | tf_op jit(solution)/shard_map/dot_general | solution.py:79
  116.1 1.4 fusion.34
  117.5 2.7 %convolution_convert_fusion.1 = bf16[2304,384]{1,0:T(8,128)(2,1)} fusion(bf16[2304,512]{1,0:T(8,128)(2,1)S(1)} %bitcast.33, bf16[512,384]{1,0:T(8,128)(2,1)S(1)} %get-tuple-element.20), kind=kOutput, calls=%fused_computation.1 | convolution fusion | flops 906854400 | bytes 4521984 | tf_op jit(solution)/shard_map/dot_general | solution.py:111
  120.2 6.9 %all-to-all-start.3 = ((bf16[8,288,384]{2,1,0:T(8,128)(2,1)}), bf16[8,288,384]{2,1,0:T(8,128)(2,1)S(1)}, u32[]{:S(2)}, u32[]{:S(2)}) async-start(bf16[8,288,384]{2,1,0:T(8,128)(2,1)} %bitcast.34), calls=%async_computation.4 | async-start | bytes 3538944 | tf_op jit(solution)/shard_map/all_to_all | solution.py:113
  127.2 5.5 %convolution_convert_fusion = bf16[2304,512]{1,0:T(8,128)(2,1)} fusion(bf16[2304,1152]{1,0:T(8,128)(2,1)} %all-gather.2.cloned.1.call-done, bf16[512,384]{1,0:T(8,128)(2,1)S(1)} %copy-done.6, bf16[512,384]{1,0:T(8,128)(2,1)S(1)} %copy-done.5), kind=kOutput, calls=%fused_computation | convolution fusion | flops 1814691840 | bytes 6684672 | tf_op jit(solution)/shard_map/dot_general | solution.py:105
  132.7 38.4 %all-to-all-done.3 = bf16[8,288,384]{2,1,0:T(8,128)(2,1)S(1)} async-done(((bf16[8,288,384]{2,1,0:T(8,128)(2,1)}), bf16[8,288,384]{2,1,0:T(8,128)(2,1)S(1)}, u32[]{:S(2)}, u32[]{:S(2)}) %all-to-all-start.3) | async-done | bytes 1769504 | tf_op jit(solution)/shard_map/all_to_all | solution.py:113
  172.1 6.8 %all-to-all-start.4 = ((f32[12,24,384]{2,1,0:T(8,128)}), f32[12,24,384]{2,1,0:T(8,128)S(1)}, u32[]{:S(2)}, u32[]{:S(2)}) async-start(f32[12,24,384]{2,1,0:T(8,128)} %bitcast.13), calls=%async_computation.5 | async-start | bytes 884736 | tf_op jit(solution)/shard_map/all_to_all | solution.py:115
  179.0 21.2 %all-to-all-done.4 = f32[12,24,384]{2,1,0:T(8,128)S(1)} async-done(((f32[12,24,384]{2,1,0:T(8,128)}), f32[12,24,384]{2,1,0:T(8,128)S(1)}, u32[]{:S(2)}, u32[]{:S(2)}) %all-to-all-start.4) | async-done | bytes 442400 | tf_op jit(solution)/shard_map/all_to_all | solution.py:115
  200.4 16.3 %all_to_all.37 = f32[12,8,384]{2,1,0:T(8,128)S(1)} all-to-all(f32[12,8,384]{2,1,0:T(8,128)S(1)} %broadcast_in_dim.19), channel_id=1, replica_groups=mesh['z'=12,'y'=8,'x'=4,'c'=2] {'z'}, dimensions={0} | all-to-all | bytes 294912 | tf_op jit(solution)/shard_map/all_to_all | solution.py:27
  217.6 5.4 %all-to-all-start.6 = ((f32[64,8,384]{2,1,0:T(8,128)}), f32[64,8,384]{2,1,0:T(8,128)S(1)}, u32[]{:S(2)}, u32[]{:S(2)}) async-start(f32[64,8,384]{2,1,0:T(8,128)} %broadcast_in_dim.20), calls=%async_computation.7 | async-start | bytes 1572864 | tf_op jit(solution)/shard_map/all_to_all | solution.py:27
  223.0 1.7 reshape.50
  224.7 21.4 %all-to-all-done.6 = f32[64,8,384]{2,1,0:T(8,128)S(1)} async-done(((f32[64,8,384]{2,1,0:T(8,128)}), f32[64,8,384]{2,1,0:T(8,128)S(1)}, u32[]{:S(2)}, u32[]{:S(2)}) %all-to-all-start.6) | async-done | bytes 786464 | tf_op jit(solution)/shard_map/all_to_all | solution.py:27
  (79 shorter events, 10.8 us)
Async XLA Ops:
  7.2 41.9 %copy-start = (f32[3,2816]{1,0:T(4,128)S(1)}, f32[3,2816]{1,0:T(4,128)}, u32[]{:S(2)}) copy-start(f32[3,2816]{1,0:T(4,128)} %param.11) | copy-start | bytes 101380
  7.2 33.2 %copy-start.3 = (bf16[512,264]{0,1:T(8,128)(2,1)S(1)}, bf16[512,264]{0,1:T(8,128)(2,1)}, u32[]{:S(2)}) copy-start(bf16[512,264]{0,1:T(8,128)(2,1)} %param.13) | copy-start | bytes 811012
  7.2 33.2 %copy-start.2 = (bf16[512,264]{0,1:T(8,128)(2,1)S(1)}, bf16[512,264]{0,1:T(8,128)(2,1)}, u32[]{:S(2)}) copy-start(bf16[512,264]{0,1:T(8,128)(2,1)} %param.7) | copy-start | bytes 811012
  7.2 100.0 %all-gather.2.cloned.1.call-start = ((), (), s32[]{:S(2)}) async-start(), calls=%async_computation.8 | async-start | bytes 5750784 | tf_op jit(solution)/shard_map/all_gather | solution.py:60
  33.0 7.2 %collective-permute-start.1 = (bf16[4,264]{1,0:T(4,128)(2,1)S(1)}, bf16[4,264]{1,0:T(4,128)(2,1)S(1)}, u32[]{:S(2)}, u32[]{:S(2)}) collective-permute-start(bf16[4,264]{1,0:T(4,128)(2,1)S(1)} %pad_maximum_fusion.4), channel_id=1, source_target_pairs={{8,0},{16,8},{24,16},{32,24},{40,32},{48,40},{56,48},{64,56},{72,6... | collective-permute-start | bytes 6344 | tf_op jit(solution)/shard_map/ppermute | solution.py:33
  34.4 5.9 %collective-permute-start = (bf16[2,264]{1,0:T(2,128)(2,1)S(1)}, bf16[2,264]{1,0:T(2,128)(2,1)S(1)}, u32[]{:S(2)}, u32[]{:S(2)}) collective-permute-start(bf16[2,264]{1,0:T(2,128)(2,1)S(1)} %copy.32), channel_id=1, source_target_pairs={{0,8},{8,16},{16,24},{24,32},{32,40},{40,48},{48,56},{56,64},{64,7... | collective-permute-start | bytes 3176 | tf_op jit(solution)/shard_map/ppermute | solution.py:33
  42.4 32.2 %all-to-all-start.1 = ((bf16[4,12,24,1152]{3,2,1,0:T(8,128)(2,1)}), bf16[4,12,24,1152]{3,2,1,0:T(8,128)(2,1)S(1)}, u32[]{:S(2)}, u32[]{:S(2)}) async-start(bf16[4,12,24,1152]{3,2,1,0:T(8,128)(2,1)} %broadcast_in_dim.17), calls=%async_computation.1 | async-start | bytes 5308416 | tf_op jit(solution)/shard_map/all_to_all | solution.py:27
  83.4 2.3 copy-start.1
  86.0 25.5 %slice-start = ((s8[5308416]{0:T(1024)(128)(4,1)}), s8[1114112]{0:T(1024)(128)(4,1)S(1)}, s32[]{:S(2)}) async-start(s8[5308416]{0:T(1024)(128)(4,1)} %bitcast.28), calls=%async_computation.10 | async-start | bytes 2228224
  107.2 4.3 %slice-start.1 = ((s8[5308416]{0:T(1024)(128)(4,1)}), s8[4194304]{0:T(1024)(128)(4,1)S(1)}, s32[]{:S(2)}) async-start(s8[5308416]{0:T(1024)(128)(4,1)} %bitcast.28), calls=%async_computation.11 | async-start | bytes 8388608
  107.2 5.2 %copy-start.8 = (bf16[2304,1152]{1,0:T(8,128)(2,1)S(1)}, bf16[2304,1152]{1,0:T(8,128)(2,1)}, u32[]{:S(2)}) copy-start(bf16[2304,1152]{1,0:T(8,128)(2,1)} %all-gather.2.cloned.1.call-done) | copy-start | bytes 15925252
  117.5 2.7 %copy-start.4 = (bf16[512,384]{1,0:T(8,128)(2,1)}, bf16[512,384]{1,0:T(8,128)(2,1)S(1)}, u32[]{:S(2)}) copy-start(bf16[512,384]{1,0:T(8,128)(2,1)S(1)} %get-tuple-element.20) | copy-start | bytes 1179652
  120.2 6.9 %copy-start.6 = (bf16[512,384]{1,0:T(8,128)(2,1)S(1)}, bf16[512,384]{1,0:T(8,128)(2,1)}, u32[]{:S(2)}) copy-start(bf16[512,384]{1,0:T(8,128)(2,1)} %get-tuple-element.23) | copy-start | bytes 1179652
  120.2 6.9 %copy-start.5 = (bf16[512,384]{1,0:T(8,128)(2,1)S(1)}, bf16[512,384]{1,0:T(8,128)(2,1)}, u32[]{:S(2)}) copy-start(bf16[512,384]{1,0:T(8,128)(2,1)} %copy-done.4) | copy-start | bytes 1179652
  120.2 50.9 %all-to-all-start.3 = ((bf16[8,288,384]{2,1,0:T(8,128)(2,1)}), bf16[8,288,384]{2,1,0:T(8,128)(2,1)S(1)}, u32[]{:S(2)}, u32[]{:S(2)}) async-start(bf16[8,288,384]{2,1,0:T(8,128)(2,1)} %bitcast.34), calls=%async_computation.4 | async-start | bytes 3538944 | tf_op jit(solution)/shard_map/all_to_all | solution.py:113
  127.1 95.9 %reduce-scatter.2.cloned.1.call-start = ((), (), s32[]{:S(2)}) async-start(), calls=%async_computation.9 | async-start | bytes 2654208 | tf_op jit(solution)/shard_map/reduce_scatter | solution.py:108
  172.1 28.1 %all-to-all-start.4 = ((f32[12,24,384]{2,1,0:T(8,128)}), f32[12,24,384]{2,1,0:T(8,128)S(1)}, u32[]{:S(2)}, u32[]{:S(2)}) async-start(f32[12,24,384]{2,1,0:T(8,128)} %bitcast.13), calls=%async_computation.5 | async-start | bytes 884736 | tf_op jit(solution)/shard_map/all_to_all | solution.py:115
  200.3 48.0 %copy-start.7 = (f32[24,384]{1,0:T(8,128)}, f32[24,384]{1,0:T(8,128)S(1)}, u32[]{:S(2)}) copy-start(f32[24,384]{1,0:T(8,128)S(1)} %reduce_sum.82) | copy-start | bytes 110596
  217.6 28.5 %all-to-all-start.6 = ((f32[64,8,384]{2,1,0:T(8,128)}), f32[64,8,384]{2,1,0:T(8,128)S(1)}, u32[]{:S(2)}, u32[]{:S(2)}) async-start(f32[64,8,384]{2,1,0:T(8,128)} %broadcast_in_dim.20), calls=%async_computation.7 | async-start | bytes 1572864 | tf_op jit(solution)/shard_map/all_to_all | solution.py:27
Sparse Core Ops, SparseCore 0:
  31.0 76.1 all-gather.1
  132.8 38.1 reduce-scatter.1
